TPU v7x, 32 devices: a whole 2x2x4 slice. The times are simulated.
32 devices in a mesh: fs: 8 (over z, y), tp: 4 (over x, core).
Axes of the slice: x: 2, y: 2, z: 4, core: 2. Of those that a mesh axis runs over, the one named last changes fastest.
Arguments:
- hidden_in: bfloat16 [512, 4096], P(None, 'tp'), may hold values from -6 to 6
- up_act: bfloat16 [512, 12288], P('tp', 'fs'), may hold values from -6 to 6
- up_val: bfloat16 [512, 12288], P('tp', 'fs'), may hold values from -6 to 6
- cotangent: bfloat16 [512, 4096], P('tp'), may hold values from -6 to 6
- w_act: bfloat16 [4096, 12288], P('tp', 'fs'), may hold values from -0.09375 to 0.09375
- w_val: bfloat16 [4096, 12288], P('tp', 'fs'), may hold values from -0.09375 to 0.09375
- w_down: bfloat16 [12288, 4096], P('fs', 'tp'), may hold values from -0.0546875 to 0.0546875
- conv_act: bfloat16 [3, 12288], P(None, 'fs'), may hold values from -3 to 3
- conv_val: bfloat16 [3, 12288], P(None, 'fs'), may hold values from -3 to 3
- bias_act: bfloat16 [12288], P('fs'), may hold values from -3 to 3
- bias_val: bfloat16 [12288], P('fs'), may hold values from -3 to 3
Outputs:
- grad_input: bfloat16 [512, 4096], P(('tp', 'fs'))
- grad_w_act: float32 [4096, 12288], P('tp', 'fs')
- grad_w_val: float32 [4096, 12288], P('tp', 'fs')
- grad_w_down: float32 [12288, 4096], P('fs', 'tp')
- grad_conv_act: float32 [3, 12288], P(None, 'fs')
- grad_conv_val: float32 [3, 12288], P(None, 'fs')
- grad_bias_act: float32 [12288], P('fs')
- grad_bias_val: float32 [12288], P('fs')
- rows_act: float32 [4096], P('tp')
- rows_val: float32 [4096], P('tp')
- rows_down: float32 [12288], P('fs')
- conv_rows: float32 [2, 3], replicated
All inputs are finite; a program needn't handle non-finite values.
Results may differ from a plain program's by a relative error of at most 0.0057.
Values may be sent and summed in bfloat16 or wider, within the bound.
A program may use at most 128 MiB of HBM per device.

v0:
```python
import jax
import jax.numpy as jnp
from jax import lax
from jax.sharding import PartitionSpec as P


def passed_along(value, axis, by):
    length = lax.axis_size(axis)
    pairs = [(i, i + by) for i in range(length) if 0 <= i + by < length]
    return lax.ppermute(value, axis, pairs)


def contract_last(left, right):
    return lax.dot_general(
        left, right, (((1,), (1,)), ((), ())), preferred_element_type=jnp.float32
    )


def contract_first(left, right):
    return lax.dot_general(
        left, right, (((0,), (0,)), ((), ())), preferred_element_type=jnp.float32
    )


def conv_ahead(extended, taps, bias, length):
    total = jnp.zeros((length, extended.shape[1]), jnp.float32) + bias.astype(jnp.float32)
    for offset in range(taps.shape[0]):
        total = total + taps[offset].astype(jnp.float32) * extended[offset : offset + length]
    return total


def conv_behind(extended, taps, length):
    reach = taps.shape[0] - 1
    total = jnp.zeros((length, extended.shape[1]), jnp.float32)
    for offset in range(taps.shape[0]):
        total = (
            total
            + taps[offset].astype(jnp.float32) * extended[reach - offset : reach - offset + length]
        )
    return total.astype(jnp.bfloat16)


def tap_grads(grad_pre, extended, tap_count):
    length = grad_pre.shape[0]
    rows = [
        jnp.sum(grad_pre * extended[offset : offset + length], axis=0)
        for offset in range(tap_count)
    ]
    return (jnp.stack(rows, 0), jnp.sum(grad_pre, axis=0))


def per_device(
    hidden_in,
    up_act,
    up_val,
    cotangent,
    w_act,
    w_val,
    w_down,
    conv_act,
    conv_val,
    bias_act,
    bias_val,
):
    local_rows = cotangent.shape[0]
    tap_count = conv_act.shape[0]
    reach = tap_count - 1
    tp_count = lax.axis_size("tp")
    fs_count = lax.axis_size("fs")
    down_whole = lax.all_gather(w_down, "tp", axis=1, tiled=True)
    prev_act, prev_val = passed_along(
        (up_act[local_rows - reach :], up_val[local_rows - reach :]), "tp", 1
    )
    ext_act = jnp.concatenate([prev_act, up_act], 0).astype(jnp.float32)
    ext_val = jnp.concatenate([prev_val, up_val], 0).astype(jnp.float32)
    pre_act = conv_ahead(ext_act, conv_act, bias_act, local_rows)
    pre_val = conv_ahead(ext_val, conv_val, bias_val, local_rows)
    gelu_act, gelu_back = jax.vjp(jax.nn.gelu, pre_act)
    mixed = (gelu_act * pre_val).astype(jnp.bfloat16)
    grad_mixed = contract_last(cotangent, down_whole).astype(jnp.bfloat16)
    grad_mixed = lax.optimization_barrier(grad_mixed).astype(jnp.float32)
    grad_pre_act = gelu_back(grad_mixed * pre_val)[0]
    grad_pre_val = grad_mixed * gelu_act
    next_act, next_val = passed_along((grad_pre_act[:reach], grad_pre_val[:reach]), "tp", -1)
    grad_up_act = conv_behind(jnp.concatenate([grad_pre_act, next_act], 0), conv_act, local_rows)
    grad_up_val = conv_behind(jnp.concatenate([grad_pre_val, next_val], 0), conv_val, local_rows)
    taps_act, sums_act = tap_grads(grad_pre_act, ext_act, tap_count)
    taps_val, sums_val = tap_grads(grad_pre_val, ext_val, tap_count)
    all_up_act, all_up_val, all_mixed = (
        lax.all_gather(grad_up_act, "tp", axis=0, tiled=True),
        lax.all_gather(grad_up_val, "tp", axis=0, tiled=True),
        lax.all_gather(mixed, "tp", axis=0, tiled=True),
    )
    cot_columns = lax.all_to_all(cotangent, "tp", split_axis=1, concat_axis=0, tiled=True)
    grad_w_act = contract_first(hidden_in, all_up_act)
    grad_w_val = contract_first(hidden_in, all_up_val)
    grad_w_down = contract_first(all_mixed, cot_columns)
    shard_rows = local_rows // fs_count
    block_rows = tp_count * shard_rows

    def select_rows(gathered):
        shaped = gathered.reshape(tp_count, fs_count, shard_rows, gathered.shape[1])
        return jnp.transpose(shaped, (1, 0, 2, 3)).reshape(
            lax.axis_size("fs") * block_rows, gathered.shape[1]
        )

    summed = lax.psum_scatter(
        contract_last(select_rows(all_up_act), w_act)
        + contract_last(select_rows(all_up_val), w_val),
        "fs",
        scatter_dimension=0,
        tiled=True,
    ).astype(jnp.bfloat16)
    grad_input = lax.all_to_all(summed, "tp", split_axis=0, concat_axis=1, tiled=True)
    down_squares = jnp.sum(grad_w_down * grad_w_down, axis=1)
    taps_act, taps_val, sums_act, sums_val, rows_down = lax.psum(
        (taps_act, taps_val, sums_act, sums_val, down_squares), "tp"
    )
    tap_squares = jnp.stack(
        [jnp.sum(taps_act * taps_act, axis=1), jnp.sum(taps_val * taps_val, axis=1)], 0
    )
    rows_act, rows_val, conv_rows = lax.psum(
        (
            jnp.sum(grad_w_act * grad_w_act, axis=1),
            jnp.sum(grad_w_val * grad_w_val, axis=1),
            tap_squares,
        ),
        "fs",
    )
    return (
        grad_input,
        grad_w_act,
        grad_w_val,
        grad_w_down,
        taps_act,
        taps_val,
        sums_act,
        sums_val,
        rows_act,
        rows_val,
        rows_down,
        conv_rows,
    )


def solution(mesh):
    return jax.shard_map(
        per_device,
        mesh=mesh,
        in_specs=(
            P(None, "tp"),
            P("tp", "fs"),
            P("tp", "fs"),
            P("tp", None),
            P("tp", "fs"),
            P("tp", "fs"),
            P("fs", "tp"),
            P(None, "fs"),
            P(None, "fs"),
            P("fs"),
            P("fs"),
        ),
        out_specs=(
            P(("tp", "fs"), None),
            P("tp", "fs"),
            P("tp", "fs"),
            P("fs", "tp"),
            P(None, "fs"),
            P(None, "fs"),
            P("fs"),
            P("fs"),
            P("tp"),
            P("tp"),
            P("fs"),
            P(),
        ),
        check_vma=False,
    )
```

profile of v0, /device:TPU:0, one launch (start us, length us, event | category | flops | bytes accessed | tf_op | source)
XLA Modules:
  0.0 296.1 jit_solution(9692622403794457745)
XLA Ops:
  8.4 2.4 collective-permute-start.1
  11.5 4.5 %collective-permute-start = (bf16[2,1536]{1,0:T(2,128)(2,1)S(1)}, bf16[2,1536]{1,0:T(2,128)(2,1)S(1)}, u32[]{:S(2)}, u32[]{:S(2)}) collective-permute-start(bf16[2,1536]{1,0:T(2,128)(2,1)S(1)} %slice.74), channel_id=1, source_target_pairs={{0,1},{1,2},{2,3},{4,5},{5,6},{6,7},{8,9},{9,10},{10,11},{12,13},{... | collective-permute-start | bytes 18440 | tf_op jit(solution)/shard_map/ppermute | solution.py:10
  19.8 2.1 maximum_convert_fusion
  21.9 72.5 %all-gather.5.cloned.1.call-done = bf16[1536,4096]{1,0:T(8,128)(2,1)} async-done(((bf16[1536,1024]{1,0:T(8,128)(2,1)}), bf16[1536,4096]{1,0:T(8,128)(2,1)}) %all-gather.5.cloned.1.call-update) | async-done | bytes 12582928 | tf_op jit(solution)/shard_map/all_gather | solution.py:70
  94.4 9.3 %convolution_convert_fusion = bf16[128,1536]{1,0:T(8,128)(2,1)S(1)} fusion(bf16[128,4096]{1,0:T(8,128)(2,1)} %param.14, bf16[1536,4096]{1,0:T(8,128)(2,1)} %all-gather.5.cloned.1.call-done), kind=kOutput, calls=%fused_computation.5 | convolution fusion | flops 1610809344 | bytes 14024704 | tf_op jit(solution)/shard_map/dot_general | solution.py:14
  107.8 2.1 multiply_reduce_fusion.8
  112.1 3.5 %collective-permute-done.2 = f32[2,1536]{1,0:T(2,128)S(1)} collective-permute-done((f32[2,1536]{1,0:T(2,128)S(1)}, f32[2,1536]{1,0:T(2,128)S(1)}, u32[]{:S(2)}, u32[]{:S(2)}) %collective-permute-start.2) | collective-permute-done | bytes 12320 | tf_op jit(solution)/shard_map/ppermute | solution.py:10
  115.5 3.0 fusion.9
  118.6 2.5 multiply_convert_fusion
  121.2 10.4 %all-gather.9.cloned.1.call-done = bf16[512,1536]{1,0:T(8,128)(2,1)} async-done(((bf16[128,1536]{1,0:T(8,128)(2,1)}), bf16[512,1536]{1,0:T(8,128)(2,1)}) %all-gather.9.cloned.1.call-update) | async-done | bytes 1572880 | tf_op jit(solution)/shard_map/all_gather | solution.py:91
  131.5 2.7 copy.34
  134.2 18.6 %all-gather.7.cloned.1.call-done = bf16[512,1536]{1,0:T(8,128)(2,1)} async-done(((bf16[128,1536]{1,0:T(8,128)(2,1)}), bf16[512,1536]{1,0:T(8,128)(2,1)}) %all-gather.7.cloned.1.call-update) | async-done | bytes 1572880 | tf_op jit(solution)/shard_map/all_gather | solution.py:90
  156.7 3.2 %convolution_add_fusion = f32[512,1024]{1,0:T(8,128)} fusion(f32[512,1024]{1,0:T(8,128)S(1)} %fusion.19, bf16[512,1536]{1,0:T(8,128)(2,1)S(1)} %bitcast.37, bf16[1024,1536]{1,0:T(8,128)(2,1)S(1)} %copy-done.17), kind=kOutput, calls=%fused_computation.6 | convolution fusion | flops 1611137024 | bytes 8912896 | tf_op jit(solution)/shard_map/dot_general | solution.py:14
  161.8 21.8 %all_to_all.38 = bf16[128,4,1024]{0,2,1:T(8,128)(2,1)S(1)} all-to-all(bf16[128,4,1024]{0,2,1:T(8,128)(2,1)S(1)} %bitcast.34), channel_id=1, replica_groups=mesh['fs'=8,'tp'=4] {'tp'}, dimensions={1} | all-to-all | bytes 2097152 | tf_op jit(solution)/shard_map/all_to_all | solution.py:94
  185.4 5.8 %multiply_reduce_fusion.1 = (f32[1024]{0:T(1024)S(1)}, f32[1024,1536]{0,1:T(8,128)}) fusion(bf16[512,1536]{1,0:T(8,128)(2,1)S(1)} %copy-done.7, bf16[512,1024]{1,0:T(8,128)(2,1)} %param.11), kind=kOutput, calls=%fused_computation.1 | convolution fusion | flops 1613757440 | bytes 8916992 | tf_op jit(solution)/shard_map/dot_general | solution.py:20
  191.1 6.7 %copy.39 = f32[1024,1536]{1,0:T(8,128)} copy(f32[1024,1536]{0,1:T(8,128)} %get-tuple-element.80) | data formatting | bytes 12582912
  197.8 6.0 %multiply_reduce_fusion = (f32[1536]{0:T(1024)S(1)}, f32[1536,1024]{0,1:T(8,128)}) fusion(bf16[512,1536]{1,0:T(8,128)(2,1)} %all-gather.11.cloned.1.call-done, bf16[512,1024]{1,0:T(8,128)(2,1)S(1)} %bitcast.39), kind=kOutput, calls=%fused_computation | convolution fusion | flops 1613756928 | bytes 8919040 | tf_op jit(solution)/shard_map/dot_general | solution.py:20
  203.8 6.7 %copy.40 = f32[1536,1024]{1,0:T(8,128)} copy(f32[1536,1024]{0,1:T(8,128)} %get-tuple-element.76) | data formatting | bytes 12582912
  210.5 11.9 %all-reduce.1 = (f32[3,1536]{1,0:T(4,128)S(1)}, f32[3,1536]{1,0:T(4,128)S(1)}, f32[1536]{0:T(1024)}, f32[1536]{0:T(1024)}, f32[1536]{0:T(1024)}) all-reduce(f32[3,1536]{1,0:T(4,128)S(1)} %pad_maximum_fusion.2, f32[3,1536]{1,0:T(4,128)S(1)} %pad_maximum_fusion.3, ...), channel_id=1, replica_groups=mesh['fs'=8,'tp'=4] {'tp'}, use_global_device_ids=true, to_apply=%region_4.0 | all-reduce | flops 13824 | bytes 110592 | tf_op jit(solution)/shard_map/psum | solution.py:116
  222.6 28.7 %reduce-scatter.2.cloned.1.call-done = f32[64,1024]{1,0:T(8,128)} async-done(((f32[512,1024]{1,0:T(8,128)}), f32[64,1024]{1,0:T(8,128)}) %reduce-scatter.2.cloned.1.call-update) | async-done | bytes 262160 | tf_op jit(solution)/shard_map/reduce_scatter | solution.py:107
  252.9 3.3 %all-to-all-start = ((bf16[4,16,1024]{2,1,0:T(8,128)(2,1)}), bf16[4,16,1024]{2,1,0:T(8,128)(2,1)S(1)}, u32[]{:S(2)}, u32[]{:S(2)}) async-start(bf16[4,16,1024]{2,1,0:T(8,128)(2,1)} %bitcast.6), calls=%async_computation.1 | async-start | bytes 262144 | tf_op jit(solution)/shard_map/all_to_all | solution.py:114
  256.3 5.7 %multiply_reduce_fusion.2 = (f32[1024]{0:T(1024)S(1)}, f32[1024,1536]{0,1:T(8,128)}) fusion(bf16[512,1536]{1,0:T(8,128)(2,1)S(1)} %copy-done.6, bf16[512,1024]{1,0:T(8,128)(2,1)} %param.11), kind=kOutput, calls=%fused_computation.2 | convolution fusion | flops 1613757440 | bytes 8916992 | tf_op jit(solution)/shard_map/dot_general | solution.py:20
  262.0 6.7 %copy.38 = f32[1024,1536]{1,0:T(8,128)} copy(f32[1024,1536]{0,1:T(8,128)} %get-tuple-element.78) | data formatting | bytes 12582912
  268.7 20.2 %all-reduce = (f32[1024]{0:T(1024)}, f32[1024]{0:T(1024)}, f32[2,3]{1,0:T(2,128)}) all-reduce(f32[1024]{0:T(1024)S(1)} %get-tuple-element.77, f32[1024]{0:T(1024)S(1)} %get-tuple-element.79, f32[2,3]{1,0:T(2,128)S(1)} %pad_maximum_fusion.4), channel_id=1, replica_groups=mesh['fs'=8,'tp'=4] {'fs'}, use_global_device_ids=true, to_apply=%region_14.0 | all-reduce | flops 2054 | bytes 16432 | tf_op jit(solution)/shard_map/psum | solution.py:122
  (79 shorter events, 21.9 us)
Async XLA Ops:
  7.2 147.1 %copy-start = (bf16[1024,1536]{1,0:T(8,128)(2,1)S(1)}, bf16[1024,1536]{1,0:T(8,128)(2,1)}, u32[]{:S(2)}) copy-start(bf16[1024,1536]{1,0:T(8,128)(2,1)} %param.15) | copy-start | bytes 9437188
  7.2 87.2 %all-gather.5.cloned.1.call-start = ((), (), s32[]{:S(2)}) async-start(), calls=%async_computation.3 | async-start | bytes 15728640 | tf_op jit(solution)/shard_map/all_gather | solution.py:70
  7.9 123.6 %all-gather.9.cloned.1.call-start = ((), (), s32[]{:S(2)}) async-start(), calls=%async_computation.5 | async-start | bytes 1966080 | tf_op jit(solution)/shard_map/all_gather | solution.py:91
  8.4 10.4 %collective-permute-start.1 = (bf16[2,1536]{1,0:T(2,128)(2,1)S(1)}, bf16[2,1536]{1,0:T(2,128)(2,1)S(1)}, u32[]{:S(2)}, u32[]{:S(2)}) collective-permute-start(bf16[2,1536]{1,0:T(2,128)(2,1)S(1)} %slice.80), channel_id=1, source_target_pairs={{0,1},{1,2},{2,3},{4,5},{5,6},{6,7},{8,9},{9,10},{10,11},{12,13},{... | collective-permute-start | bytes 18440 | tf_op jit(solution)/shard_map/ppermute | solution.py:10
  11.5 8.3 %collective-permute-start = (bf16[2,1536]{1,0:T(2,128)(2,1)S(1)}, bf16[2,1536]{1,0:T(2,128)(2,1)S(1)}, u32[]{:S(2)}, u32[]{:S(2)}) collective-permute-start(bf16[2,1536]{1,0:T(2,128)(2,1)S(1)} %slice.74), channel_id=1, source_target_pairs={{0,1},{1,2},{2,3},{4,5},{5,6},{6,7},{8,9},{9,10},{10,11},{12,13},{... | collective-permute-start | bytes 18440 | tf_op jit(solution)/shard_map/ppermute | solution.py:10
  21.9 81.8 %copy-start.11 = (f32[1536]{0:T(1024)S(1)}, f32[1536]{0:T(1024)}, u32[]{:S(2)}) copy-start(f32[1536]{0:T(1024)} %get-tuple-element.61) | copy-start | bytes 18436
  21.9 81.8 %copy-start.12 = (f32[1536]{0:T(1024)S(1)}, f32[1536]{0:T(1024)}, u32[]{:S(2)}) copy-start(f32[1536]{0:T(1024)} %convert_element_type.52) | copy-start | bytes 18436
  94.4 9.3 %copy-start.2 = (f32[130,1536]{1,0:T(8,128)S(1)}, f32[130,1536]{1,0:T(8,128)}, u32[]{:S(2)}) copy-start(f32[130,1536]{1,0:T(8,128)} %maximum_convert_fusion.1) | copy-start | bytes 2396164
  94.4 9.3 %copy-start.3 = (f32[130,1536]{1,0:T(8,128)S(1)}, f32[130,1536]{1,0:T(8,128)}, u32[]{:S(2)}) copy-start(f32[130,1536]{1,0:T(8,128)} %maximum_convert_fusion) | copy-start | bytes 2396164
  103.8 2.2 copy-start.13
  103.8 2.3 copy-start.16
  104.7 5.2 %copy-start.4 = (f32[128,1536]{1,0:T(8,128)}, f32[128,1536]{1,0:T(8,128)S(1)}, u32[]{:S(2)}) copy-start(f32[128,1536]{1,0:T(8,128)S(1)} %get-tuple-element.71) | copy-start | bytes 2359300
  104.7 3.1 %collective-permute-start.3 = (f32[2,1536]{1,0:T(2,128)S(1)}, f32[2,1536]{1,0:T(2,128)S(1)}, u32[]{:S(2)}, u32[]{:S(2)}) collective-permute-start(f32[2,1536]{1,0:T(2,128)S(1)} %slice.101), channel_id=1, source_target_pairs={{1,0},{2,1},{3,2},{5,4},{6,5},{7,6},{9,8},{10,9},{11,10},{13,12},{... | collective-permute-start | bytes 36872 | tf_op jit(solution)/shard_map/ppermute | solution.py:10
  109.9 42.9 %all-gather.7.cloned.1.call-start = ((), (), s32[]{:S(2)}) async-start(), calls=%async_computation.4 | async-start | bytes 1966080 | tf_op jit(solution)/shard_map/all_gather | solution.py:90
  110.8 4.8 %collective-permute-start.2 = (f32[2,1536]{1,0:T(2,128)S(1)}, f32[2,1536]{1,0:T(2,128)S(1)}, u32[]{:S(2)}, u32[]{:S(2)}) collective-permute-start(f32[2,1536]{1,0:T(2,128)S(1)} %slice.98), channel_id=1, source_target_pairs={{1,0},{2,1},{3,2},{5,4},{6,5},{7,6},{9,8},{10,9},{11,10},{13,12},{... | collective-permute-start | bytes 36872 | tf_op jit(solution)/shard_map/ppermute | solution.py:10
  118.5 79.3 %all-gather.11.cloned.1.call-start = ((), (), s32[]{:S(2)}) async-start(), calls=%async_computation.7 | async-start | bytes 1966080 | tf_op jit(solution)/shard_map/all_gather | solution.py:92
  121.1 130.2 %reduce-scatter.2.cloned.1.call-start = ((), (), s32[]{:S(2)}) async-start(), calls=%async_computation.6 | async-start | bytes 2359296 | tf_op jit(solution)/shard_map/reduce_scatter | solution.py:107
  154.3 2.4 copy-start.17
  191.1 6.7 %copy-start.9 = (bf16[4,128,1024]{2,1,0:T(8,128)(2,1)S(1)}, bf16[4,128,1024]{2,1,0:T(8,128)(2,1)}, u32[]{:S(2)}) copy-start(bf16[4,128,1024]{2,1,0:T(8,128)(2,1)} %copy.37) | copy-start | bytes 3145732
  203.8 52.5 %copy-start.6 = (bf16[512,1536]{1,0:T(8,128)(2,1)S(1)}, bf16[512,1536]{1,0:T(8,128)(2,1)}, u32[]{:S(2)}) copy-start(bf16[512,1536]{1,0:T(8,128)(2,1)} %all-gather.7.cloned.1.call-done) | copy-start | bytes 4718596
  222.4 39.5 %copy-start.14 = (f32[3,1536]{1,0:T(4,128)}, f32[3,1536]{1,0:T(4,128)S(1)}, u32[]{:S(2)}) copy-start(f32[3,1536]{1,0:T(4,128)S(1)} %get-tuple-element.65) | copy-start | bytes 55300
  222.4 39.5 %copy-start.15 = (f32[3,1536]{1,0:T(4,128)}, f32[3,1536]{1,0:T(4,128)S(1)}, u32[]{:S(2)}) copy-start(f32[3,1536]{1,0:T(4,128)S(1)} %get-tuple-element.66) | copy-start | bytes 55300
  252.9 35.9 %all-to-all-start = ((bf16[4,16,1024]{2,1,0:T(8,128)(2,1)}), bf16[4,16,1024]{2,1,0:T(8,128)(2,1)S(1)}, u32[]{:S(2)}, u32[]{:S(2)}) async-start(bf16[4,16,1024]{2,1,0:T(8,128)(2,1)} %bitcast.6), calls=%async_computation.1 | async-start | bytes 262144 | tf_op jit(solution)/shard_map/all_to_all | solution.py:114
  262.0 27.5 %copy-start.1 = (bf16[1024,1536]{1,0:T(8,128)(2,1)S(1)}, bf16[1024,1536]{1,0:T(8,128)(2,1)}, u32[]{:S(2)}) copy-start(bf16[1024,1536]{1,0:T(8,128)(2,1)} %param.15) | copy-start | bytes 9437188
  (4 other events, 6.1 us)
Sparse Core Ops, SparseCore 0:
  9.6 84.7 all-gather.4
  110.0 21.4 all-gather.8
  133.1 19.6 all-gather.6
  154.2 24.6 all-gather.10
  182.2 68.9 reduce-scatter.1
where the time goes:
time: 297 us; the launch traced here: 296 us
  waiting for transfers between devices  136 us (46%)
  blocking collectives  53.9 us (18%)
  matrix products  31.7 us (11%)
  local copies, waits for them, and re-layouts  31 us (10%)
  other arithmetic  16.2 us (5%)
  between operations  14.1 us (5%)
  starting transfers between devices  13 us (4%)
    all_gather x1, waiting for transfers between devices, per_device(): down_whole = lax.all_gather(w_down, 'tp', axis=1, tiled=True)  72.5 us
    reduce_scatter x1, waiting for transfers between devices, per_device(): lax.psum_scatter(contract_last(select_rows(all_up_act), w_act) + contract...  28.7 us
    unnamed x40, local copies, waits for them, and re-layouts  23.3 us
    all_to_all x1, blocking collectives, per_device(): lax.all_to_all(cotangent, 'tp', split_axis=1, concat_axis=0, tiled=True)  21.8 us
    psum x1, blocking collectives, per_device(): lax.psum((jnp.sum(grad_w_act * grad_w_act, axis=1), jnp.sum(grad_w_val *...  20.2 us
    all_gather x1, waiting for transfers between devices, per_device(): lax.all_gather(grad_up_act, 'tp', axis=0, tiled=True)  18.6 us
    dot_general x3, matrix products, contract_first(): lax.dot_general(left, right, (((0,), (0,)), ((), ())), preferred_element_...  17.5 us
    dot_general x3, matrix products, contract_last(): lax.dot_general(left, right, (((1,), (1,)), ((), ())), preferred_element_...  14.3 us
  transfers between devices with their start and end apart: 10, of which 6 were waited for; matrix products, arithmetic and copies ran while one was open for 21% of the time, Pallas kernels for 0%

commit v1 on v0

--- a/solution.py
+++ b/solution.py
@@ -67,7 +67,12 @@
     reach = tap_count - 1
     tp_count = lax.axis_size("tp")
     fs_count = lax.axis_size("fs")
-    down_whole = lax.all_gather(w_down, "tp", axis=1, tiled=True)
+    ring = [w_down]
+    for hop in range(3):
+        ring.append(lax.ppermute(ring[-1], "tp", [(dev, (dev + 1) % 4) for dev in range(4)]))
+    down_whole = jnp.roll(
+        jnp.concatenate(ring[::-1], axis=1), (lax.axis_index("tp") + 1) * ring[0].shape[1], axis=1
+    )
     prev_act, prev_val = passed_along(
         (up_act[local_rows - reach :], up_val[local_rows - reach :]), "tp", 1
     )

time: 297 us -> 373 us (1.26)
  local copies, waits for them, and re-layouts: 31 us -> 71 us
  waiting for transfers between devices: 136 us -> 160 us
  other arithmetic: 16.2 us -> 31 us
    ppermute x0 -> x3, waiting for transfers between devices: none -> 91.3 us  [per_device(): lax.ppermute(ring[-1], 'tp', [(dev, (dev + 1) % 4) for dev in range(4)])]
    all_gather x1 -> x0, waiting for transfers between devices: 72.5 us -> none  [per_device(): down_whole = lax.all_gather(w_down, 'tp', axis=1, tiled=True)]
    unnamed x40 -> x63, local copies, waits for them, and re-layouts: 23.3 us -> 48.6 us
    reduce_sum x2, other arithmetic: 3.01 us -> 13.8 us  [tap_grads(): jnp.sum(grad_pre * extended[offset:offset + length], axis=0)]
    ppermute x4, waiting for transfers between devices: 5.15 us -> 13.6 us  [passed_along(): return lax.ppermute(value, axis, pairs)]
    all_gather x0 -> x2, local copies, waits for them, and re-layouts: none -> 5.15 us  [the longest x1 2.58 us: per_device(): lax.all_gather(grad_up_val, 'tp', axis=0, tiled=True)]
    reshape x2 -> x0, local copies, waits for them, and re-layouts: 4.18 us -> none  [select_rows(): shaped = gathered.reshape(tp_count, fs_count, shard_rows, gathered.shape[1])]
    transpose x0 -> x2, local copies, waits for them, and re-layouts: none -> 4.18 us  [select_rows(): jnp.transpose(shaped, (1, 0, 2, 3))]
  transfers between devices with their start and end apart: 10 -> 12, of which waited for: 6 -> 8; matrix products, arithmetic and copies ran while one was open for 21% -> 21% of each run, Pallas kernels for 0% -> 0%
where the time goes in v1:
time: 373 us; the launch traced here: 371 us
  waiting for transfers between devices  160 us (43%)
  local copies, waits for them, and re-layouts  71 us (19%)
  blocking collectives  52.7 us (14%)
  other arithmetic  31 us (8%)
  matrix products  28.9 us (8%)
  between operations  14.2 us (4%)
  starting transfers between devices  13.9 us (4%)
    ppermute x3, waiting for transfers between devices, per_device(): lax.ppermute(ring[-1], 'tp', [(dev, (dev + 1) % 4) for dev in range(4)])  91.3 us
    unnamed x63, local copies, waits for them, and re-layouts  48.6 us
    reduce_scatter x1, waiting for transfers between devices, per_device(): lax.psum_scatter(contract_last(select_rows(all_up_act), w_act) + contract...  28.9 us
    all_to_all x1, blocking collectives, per_device(): lax.all_to_all(cotangent, 'tp', split_axis=1, concat_axis=0, tiled=True)  20.5 us
    psum x1, blocking collectives, per_device(): lax.psum((jnp.sum(grad_w_act * grad_w_act, axis=1), jnp.sum(grad_w_val *...  20.2 us
    dot_general x3, matrix products, contract_first(): lax.dot_general(left, right, (((0,), (0,)), ((), ())), preferred_element_...  17.4 us
    all_gather x1, waiting for transfers between devices, per_device(): lax.all_gather(grad_up_act, 'tp', axis=0, tiled=True)  16.7 us
    reduce_sum x2, other arithmetic, tap_grads(): jnp.sum(grad_pre * extended[offset:offset + length], axis=0)  13.8 us
  transfers between devices with their start and end apart: 12, of which 8 were waited for; matrix products, arithmetic and copies ran while one was open for 21% of the time, Pallas kernels for 0%

profile of v1, /device:TPU:0, one launch (start us, length us, event | category | flops | bytes accessed | tf_op | source)
XLA Modules:
  0.0 371.3 jit_solution(12499299515752738530)
XLA Ops:
  7.8 37.1 %collective-permute-done = bf16[1536,1024]{1,0:T(8,128)(2,1)S(1)} collective-permute-done((bf16[1536,1024]{1,0:T(8,128)(2,1)}, bf16[1536,1024]{1,0:T(8,128)(2,1)S(1)}, u32[]{:S(2)}, u32[]{:S(2)}) %collective-permute-start) | collective-permute-done | bytes 3145760 | tf_op jit(solution)/shard_map/ppermute | solution.py:72
  46.6 36.8 %collective-permute-done.1 = bf16[1536,1024]{1,0:T(8,128)(2,1)} collective-permute-done((bf16[1536,1024]{1,0:T(8,128)(2,1)S(1)}, bf16[1536,1024]{1,0:T(8,128)(2,1)}, u32[]{:S(2)}, u32[]{:S(2)}) %collective-permute-start.1) | collective-permute-done | bytes 3145760 | tf_op jit(solution)/shard_map/ppermute | solution.py:72
  85.0 5.1 %collective-permute-start.3 = (bf16[2,1536]{0,1:T(8,128)(2,1)}, bf16[2,1536]{0,1:T(8,128)(2,1)}, u32[]{:S(2)}, u32[]{:S(2)}) collective-permute-start(bf16[2,1536]{0,1:T(8,128)(2,1)} %copy.57), channel_id=1, source_target_pairs={{0,1},{1,2},{2,3},{4,5},{5,6},{6,7},{8,9},{9,10},{10,11},{12,13},{... | collective-permute-start | bytes 18440 | tf_op jit(solution)/shard_map/ppermute | solution.py:10
  102.8 17.5 %collective-permute-done.2 = bf16[1536,1024]{1,0:T(8,128)(2,1)} collective-permute-done((bf16[1536,1024]{1,0:T(8,128)(2,1)}, bf16[1536,1024]{1,0:T(8,128)(2,1)}, u32[]{:S(2)}, u32[]{:S(2)}) %collective-permute-start.2) | collective-permute-done | bytes 3145760 | tf_op jit(solution)/shard_map/ppermute | solution.py:72
  120.3 3.9 %constant_dynamic-update-slice_fusion.7 = bf16[1536,8192]{1,0:T(8,128)(2,1)} fusion(bf16[1536,1024]{1,0:T(8,128)(2,1)} %collective-permute-done.2), kind=kLoop, calls=%fused_computation.61 | loop fusion | bytes 6291456
  124.2 4.0 %constant_dynamic-update-slice_fusion.6 = bf16[1536,8192]{1,0:T(8,128)(2,1)} fusion(bf16[1536,8192]{1,0:T(8,128)(2,1)} %constant_dynamic-update-slice_fusion.7, bf16[1536,1024]{1,0:T(8,128)(2,1)} %collective-permute-done.1), kind=kLoop, calls=%fused_computation.60 | loop fusion | bytes 6291456
  144.7 6.5 %fusion.5 = bf16[128,1536]{0,1:T(8,128)(2,1)S(1)} fusion(bf16[128,4096]{1,0:T(8,128)(2,1)S(1)} %copy-done.10, bf16[1536,8192]{1,0:T(8,128)(2,1)} %constant_dynamic-update-slice_fusion, s32[]{:T(128)S(6)} %select_n.14), kind=kOutput, calls=%fused_computation.8 | convolution fusion | flops 1610809344 | bytes 14024708 | tf_op jit(solution)/shard_map/dot_general | solution.py:14
  151.3 4.1 %multiply_reduce_fusion.5 = (f32[1536]{0:T(1024)}, f32[1536]{0:T(1024)}, f32[1536]{0:T(1024)}, f32[1536]{0:T(1024)}, f32[128,1536]{0,1:T(8,128)}, /*index=5*/f32[128,1536]{0,1:T(8,128)}) fusion(f32[130,1536]{0,1:T(8,128)S(1)} %maximum_convert_fusion, bf16[128,1536]{0,1:T(8,128)(2,1)S(1)} %fusion.5, f32[130,1536]{0,1:T(8,128)S(1)} %maximum_convert_fusion.1, ...), kind=kLoop, calls=%fused_computation.42 | loop fusion | flops 4515840 | bytes 6733824 | tf_op jit(solution)/shard_map/reduce_sum | solution.py:46
  161.4 9.1 %collective-permute-done.6 = f32[2,1536]{1,0:T(2,128)} collective-permute-done((f32[2,1536]{1,0:T(2,128)}, f32[2,1536]{1,0:T(2,128)}, u32[]{:S(2)}, u32[]{:S(2)}) %collective-permute-start.6) | collective-permute-done | bytes 12320 | tf_op jit(solution)/shard_map/ppermute | solution.py:10
  172.4 9.6 %multiply_reduce_fusion.8 = (f32[1536]{0:T(1024)}, f32[1536]{0:T(1024)}, f32[1536]{0:T(1024)}, f32[1536]{0:T(1024)}, f32[128,1536]{0,1:T(8,128)}, /*index=5*/f32[128,1536]{0,1:T(8,128)}, bf16[128,1536]{0,1:T(8,128)(2,1)}) fusion(f32[130,1536]{0,1:T(8,128)} %copy-done.3, f32[128,1536]{0,1:T(8,128)} %get-tuple-element.83, bf16[128,1536]{0,1:T(8,128)(2,1)S(1)} %fusion.5, ...), kind=kLoop, calls=%fused_computation.45 | loop fusion | flops 8251392 | bytes 8712192 | tf_op jit(solution)/shard_map/reduce_sum | solution.py:46
  184.8 4.4 %collective-permute-done.5 = f32[2,1536]{1,0:T(2,128)S(1)} collective-permute-done((f32[2,1536]{1,0:T(2,128)S(1)}, f32[2,1536]{1,0:T(2,128)S(1)}, u32[]{:S(2)}, u32[]{:S(2)}) %collective-permute-start.5) | collective-permute-done | bytes 12320 | tf_op jit(solution)/shard_map/ppermute | solution.py:10
  190.5 4.4 %fusion.23 = bf16[128,1536]{0,1:T(8,128)(2,1)} fusion(f32[128,1536]{0,1:T(8,128)} %get-tuple-element.84, f32[2,1536]{0,1:T(8,128)} %copy.62, f32[1536]{0:T(1024)S(1)} %get-tuple-element.72, f32[1536]{0:T(1024)} %get-tuple-element.73, f32[1536]{0:T(1024)S(1)} %get-tuple-element.71), kind=kLoop, calls=%fused_computation.33 | loop fusion | flops 1572864 | bytes 1210368 | tf_op jit(solution)/shard_map/convert_element_type | solution.py:40
  197.6 9.1 %all-gather.6.cloned.1.call-done = bf16[512,1536]{0,1:T(8,128)(2,1)} async-done(((bf16[128,1536]{0,1:T(8,128)(2,1)}), bf16[512,1536]{0,1:T(8,128)(2,1)}) %all-gather.6.cloned.1.call-update) | async-done | bytes 1572880 | tf_op jit(solution)/shard_map/all_gather | solution.py:96
  212.0 16.7 %all-gather.4.cloned.1.call-done = bf16[512,1536]{0,1:T(8,128)(2,1)} async-done(((bf16[128,1536]{0,1:T(8,128)(2,1)}), bf16[512,1536]{0,1:T(8,128)(2,1)}) %all-gather.4.cloned.1.call-update) | async-done | bytes 1572880 | tf_op jit(solution)/shard_map/all_gather | solution.py:95
  239.1 20.5 %all_to_all.38 = bf16[128,4,1024]{0,2,1:T(8,128)(2,1)S(1)} all-to-all(bf16[128,4,1024]{0,2,1:T(8,128)(2,1)S(1)} %bitcast.41), channel_id=1, replica_groups=mesh['fs'=8,'tp'=4] {'tp'}, dimensions={1} | all-to-all | bytes 2097152 | tf_op jit(solution)/shard_map/all_to_all | solution.py:99
  260.4 6.0 %multiply_reduce_fusion = (f32[1536]{0:T(1024)S(1)}, f32[1536,1024]{0,1:T(8,128)}) fusion(bf16[512,1536]{0,1:T(8,128)(2,1)} %all-gather.8.cloned.1.call-done, bf16[512,1024]{1,0:T(8,128)(2,1)S(1)} %bitcast.44), kind=kOutput, calls=%fused_computation.2 | convolution fusion | flops 1613756928 | bytes 8919040 | tf_op jit(solution)/shard_map/dot_general | solution.py:20
  266.4 6.7 %copy.74 = f32[1536,1024]{1,0:T(8,128)} copy(f32[1536,1024]{0,1:T(8,128)} %get-tuple-element.88) | data formatting | bytes 12582912
  273.0 5.7 %multiply_reduce_fusion.1 = (f32[1024]{0:T(1024)S(1)}, f32[1024,1536]{0,1:T(8,128)}) fusion(bf16[512,1536]{0,1:T(8,128)(2,1)S(1)} %copy-done.8, bf16[512,1024]{1,0:T(8,128)(2,1)} %param.11), kind=kOutput, calls=%fused_computation.3 | convolution fusion | flops 1613757440 | bytes 8916992 | tf_op jit(solution)/shard_map/dot_general | solution.py:20
  278.8 6.7 %copy.73 = f32[1024,1536]{1,0:T(8,128)} copy(f32[1024,1536]{0,1:T(8,128)} %get-tuple-element.92) | data formatting | bytes 12582912
  285.5 12.0 %all-reduce.1 = (f32[3,1536]{1,0:T(4,128)S(1)}, f32[3,1536]{1,0:T(4,128)S(1)}, f32[1536]{0:T(1024)}, f32[1536]{0:T(1024)}, f32[1536]{0:T(1024)}) all-reduce(f32[3,1536]{1,0:T(4,128)S(1)} %pad_maximum_fusion.2, f32[3,1536]{1,0:T(4,128)S(1)} %pad_maximum_fusion.3, f32[1536]{0:T(1024)S(1)} %copy-done.14, ...), channel_id=1, replica_groups=mesh['fs'=8,'tp'=4] {'tp'}, use_global_device_ids=true, to_apply=%region_4.5 | all-reduce | flops 13824 | bytes 110592 | tf_op jit(solution)/shard_map/psum | solution.py:121
  297.7 28.9 %reduce-scatter.2.cloned.1.call-done = f32[64,1024]{1,0:T(8,128)} async-done(((f32[512,1024]{1,0:T(8,128)}), f32[64,1024]{1,0:T(8,128)}) %reduce-scatter.2.cloned.1.call-update) | async-done | bytes 262160 | tf_op jit(solution)/shard_map/reduce_scatter | solution.py:112
  331.5 5.7 %multiply_reduce_fusion.2 = (f32[1024]{0:T(1024)S(1)}, f32[1024,1536]{0,1:T(8,128)}) fusion(bf16[512,1536]{0,1:T(8,128)(2,1)S(1)} %copy-done.7, bf16[512,1024]{1,0:T(8,128)(2,1)} %param.11), kind=kOutput, calls=%fused_computation.4 | convolution fusion | flops 1613757440 | bytes 8916992 | tf_op jit(solution)/shard_map/dot_general | solution.py:20
  337.2 6.7 %copy.72 = f32[1024,1536]{1,0:T(8,128)} copy(f32[1024,1536]{0,1:T(8,128)} %get-tuple-element.90) | data formatting | bytes 12582912
  343.9 20.2 %all-reduce = (f32[1024]{0:T(1024)}, f32[1024]{0:T(1024)}, f32[2,3]{1,0:T(2,128)}) all-reduce(f32[1024]{0:T(1024)S(1)} %get-tuple-element.89, f32[1024]{0:T(1024)S(1)} %get-tuple-element.91, f32[2,3]{1,0:T(2,128)S(1)} %pad_maximum_fusion.4), channel_id=1, replica_groups=mesh['fs'=8,'tp'=4] {'fs'}, use_global_device_ids=true, to_apply=%region_14.15 | all-reduce | flops 2054 | bytes 16432 | tf_op jit(solution)/shard_map/psum | solution.py:127
  (112 shorter events, 69.7 us)
Async XLA Ops:
  7.2 225.6 %copy-start = (bf16[1024,1536]{1,0:T(8,128)(2,1)S(1)}, bf16[1024,1536]{1,0:T(8,128)(2,1)}, u32[]{:S(2)}) copy-start(bf16[1024,1536]{1,0:T(8,128)(2,1)} %param.15) | copy-start | bytes 9437188
  7.2 199.5 %all-gather.6.cloned.1.call-start = ((), (), s32[]{:S(2)}) async-start(), calls=%async_computation.4 | async-start | bytes 1966080 | tf_op jit(solution)/shard_map/all_gather | solution.py:96
  7.2 37.6 %collective-permute-start = (bf16[1536,1024]{1,0:T(8,128)(2,1)}, bf16[1536,1024]{1,0:T(8,128)(2,1)S(1)}, u32[]{:S(2)}, u32[]{:S(2)}) collective-permute-start(bf16[1536,1024]{1,0:T(8,128)(2,1)} %param.17), channel_id=1, source_target_pairs={{0,1},{1,2},{2,3},{3,0},{4,5},{5,6},{6,7},{7,4},{8,9},{9,10},{10,1... | collective-permute-start | bytes 9437192 | tf_op jit(solution)/shard_map/ppermute | solution.py:72
  46.5 36.8 %collective-permute-start.1 = (bf16[1536,1024]{1,0:T(8,128)(2,1)S(1)}, bf16[1536,1024]{1,0:T(8,128)(2,1)}, u32[]{:S(2)}, u32[]{:S(2)}) collective-permute-start(bf16[1536,1024]{1,0:T(8,128)(2,1)S(1)} %collective-permute-done), channel_id=1, source_target_pairs={{0,1},{1,2},{2,3},{3,0},{4,5},{5,6},{6,7},{7,4},{8,9},{9,10},{10,1... | collective-permute-start | bytes 9437192 | tf_op jit(solution)/shard_map/ppermute | solution.py:72
  83.3 37.0 %collective-permute-start.2 = (bf16[1536,1024]{1,0:T(8,128)(2,1)}, bf16[1536,1024]{1,0:T(8,128)(2,1)}, u32[]{:S(2)}, u32[]{:S(2)}) collective-permute-start(bf16[1536,1024]{1,0:T(8,128)(2,1)} %collective-permute-done.1), channel_id=1, source_target_pairs={{0,1},{1,2},{2,3},{3,0},{4,5},{5,6},{6,7},{7,4},{8,9},{9,10},{10,1... | collective-permute-start | bytes 9437192 | tf_op jit(solution)/shard_map/ppermute | solution.py:72
  85.0 14.7 %collective-permute-start.3 = (bf16[2,1536]{0,1:T(8,128)(2,1)}, bf16[2,1536]{0,1:T(8,128)(2,1)}, u32[]{:S(2)}, u32[]{:S(2)}) collective-permute-start(bf16[2,1536]{0,1:T(8,128)(2,1)} %copy.57), channel_id=1, source_target_pairs={{0,1},{1,2},{2,3},{4,5},{5,6},{6,7},{8,9},{9,10},{10,11},{12,13},{... | collective-permute-start | bytes 18440 | tf_op jit(solution)/shard_map/ppermute | solution.py:10
  91.8 9.4 %collective-permute-start.4 = (bf16[2,1536]{0,1:T(8,128)(2,1)}, bf16[2,1536]{0,1:T(8,128)(2,1)}, u32[]{:S(2)}, u32[]{:S(2)}) collective-permute-start(bf16[2,1536]{0,1:T(8,128)(2,1)} %copy.59), channel_id=1, source_target_pairs={{0,1},{1,2},{2,3},{4,5},{5,6},{6,7},{8,9},{9,10},{10,11},{12,13},{... | collective-permute-start | bytes 18440 | tf_op jit(solution)/shard_map/ppermute | solution.py:10
  101.2 50.0 %copy-start.2 = (f32[130,1536]{0,1:T(8,128)}, f32[130,1536]{0,1:T(8,128)S(1)}, u32[]{:S(2)}) copy-start(f32[130,1536]{0,1:T(8,128)S(1)} %maximum_convert_fusion) | copy-start | bytes 2396164
  102.8 48.4 %copy-start.3 = (f32[130,1536]{0,1:T(8,128)}, f32[130,1536]{0,1:T(8,128)S(1)}, u32[]{:S(2)}) copy-start(f32[130,1536]{0,1:T(8,128)S(1)} %maximum_convert_fusion.1) | copy-start | bytes 2396164
  157.4 13.2 %collective-permute-start.6 = (f32[2,1536]{1,0:T(2,128)}, f32[2,1536]{1,0:T(2,128)}, u32[]{:S(2)}, u32[]{:S(2)}) collective-permute-start(f32[2,1536]{1,0:T(2,128)} %copy.65), channel_id=1, source_target_pairs={{1,0},{2,1},{3,2},{5,4},{6,5},{7,6},{9,8},{10,9},{11,10},{13,12},{... | collective-permute-start | bytes 36872 | tf_op jit(solution)/shard_map/ppermute | solution.py:10
  182.1 46.6 %all-gather.4.cloned.1.call-start = ((), (), s32[]{:S(2)}) async-start(), calls=%async_computation.3 | async-start | bytes 1966080 | tf_op jit(solution)/shard_map/all_gather | solution.py:95
  183.5 5.7 %collective-permute-start.5 = (f32[2,1536]{1,0:T(2,128)S(1)}, f32[2,1536]{1,0:T(2,128)S(1)}, u32[]{:S(2)}, u32[]{:S(2)}) collective-permute-start(f32[2,1536]{1,0:T(2,128)S(1)} %copy.61), channel_id=1, source_target_pairs={{1,0},{2,1},{3,2},{5,4},{6,5},{7,6},{9,8},{10,9},{11,10},{13,12},{... | collective-permute-start | bytes 36872 | tf_op jit(solution)/shard_map/ppermute | solution.py:10
  194.9 65.5 %all-gather.8.cloned.1.call-start = ((), (), s32[]{:S(2)}) async-start(), calls=%async_computation.6 | async-start | bytes 1966080 | tf_op jit(solution)/shard_map/all_gather | solution.py:97
  197.4 129.1 %reduce-scatter.2.cloned.1.call-start = ((), (), s32[]{:S(2)}) async-start(), calls=%async_computation.5 | async-start | bytes 2359296 | tf_op jit(solution)/shard_map/reduce_scatter | solution.py:112
  238.4 21.8 %copy-start.16 = (f32[1536]{0:T(1024)S(1)}, f32[1536]{0:T(1024)}, u32[]{:S(2)}) copy-start(f32[1536]{0:T(1024)} %get-tuple-element.62) | copy-start | bytes 18436
  238.4 21.8 %copy-start.15 = (f32[1536]{0:T(1024)S(1)}, f32[1536]{0:T(1024)}, u32[]{:S(2)}) copy-start(f32[1536]{0:T(1024)} %get-tuple-element.61) | copy-start | bytes 18436
  238.4 21.9 %copy-start.20 = (f32[1536]{0:T(1024)S(1)}, f32[1536]{0:T(1024)}, u32[]{:S(2)}) copy-start(f32[1536]{0:T(1024)} %get-tuple-element.63) | copy-start | bytes 18436
  238.4 21.9 %copy-start.19 = (f32[1536]{0:T(1024)S(1)}, f32[1536]{0:T(1024)}, u32[]{:S(2)}) copy-start(f32[1536]{0:T(1024)} %get-tuple-element.65) | copy-start | bytes 18436
  238.4 21.9 %copy-start.18 = (f32[1536]{0:T(1024)S(1)}, f32[1536]{0:T(1024)}, u32[]{:S(2)}) copy-start(f32[1536]{0:T(1024)} %get-tuple-element.64) | copy-start | bytes 18436
  278.8 52.7 %copy-start.7 = (bf16[512,1536]{0,1:T(8,128)(2,1)S(1)}, bf16[512,1536]{0,1:T(8,128)(2,1)}, u32[]{:S(2)}) copy-start(bf16[512,1536]{0,1:T(8,128)(2,1)} %all-gather.4.cloned.1.call-done) | copy-start | bytes 4718596
  297.5 39.7 %copy-start.22 = (f32[3,1536]{1,0:T(4,128)}, f32[3,1536]{1,0:T(4,128)S(1)}, u32[]{:S(2)}) copy-start(f32[3,1536]{1,0:T(4,128)S(1)} %get-tuple-element.77) | copy-start | bytes 55300
  297.5 39.7 %copy-start.23 = (f32[3,1536]{1,0:T(4,128)}, f32[3,1536]{1,0:T(4,128)S(1)}, u32[]{:S(2)}) copy-start(f32[3,1536]{1,0:T(4,128)S(1)} %get-tuple-element.78) | copy-start | bytes 55300
  328.2 35.9 %all-to-all-start = ((bf16[4,16,1024]{2,1,0:T(8,128)(2,1)}), bf16[4,16,1024]{2,1,0:T(8,128)(2,1)S(1)}, u32[]{:S(2)}, u32[]{:S(2)}) async-start(bf16[4,16,1024]{2,1,0:T(8,128)(2,1)} %bitcast.7), calls=%async_computation.1 | async-start | bytes 262144 | tf_op jit(solution)/shard_map/all_to_all | solution.py:119
  337.2 27.6 %copy-start.1 = (bf16[1024,1536]{1,0:T(8,128)(2,1)S(1)}, bf16[1024,1536]{1,0:T(8,128)(2,1)}, u32[]{:S(2)}) copy-start(bf16[1024,1536]{1,0:T(8,128)(2,1)} %param.15) | copy-start | bytes 9437188
  (13 other events, 73.1 us)
Sparse Core Ops, SparseCore 0:
  182.2 24.4 all-gather.5
  208.8 19.8 all-gather.3
  230.2 23.5 all-gather.7
  257.2 69.3 reduce-scatter.1
